TPU v7x, 32 devices: a whole 2x2x4 slice. The times are simulated.
32 devices in a mesh: sp: 8 (over z, y), tp: 4 (over x, core).
Axes of the slice: x: 2, y: 2, z: 4, core: 2. Of those that a mesh axis runs over, the one named last changes fastest.
Arguments:
- hidden: bfloat16 [16, 512, 1024], P(None, 'sp'), may hold values from -0.09375 to 0.09375
- value_weight: bfloat16 [1024, 1024], P(None, 'tp'), may hold values from -0.75 to 0.75
- queries: bfloat16 [16, 8, 512, 64], P(None, 'tp', 'sp'), may hold values from -0.1875 to 0.1875
- key_vectors: bfloat16 [16, 8, 512, 64], P(None, 'tp', 'sp'), may hold values from -0.1875 to 0.1875
- forward_decay: float32 [16, 8, 512, 64], P(None, 'tp', 'sp'), may hold values from -0.005859375 to -1.953125e-05
- backward_decay: float32 [16, 8, 512, 64], P(None, 'tp', 'sp'), may hold values from -0.005859375 to -1.953125e-05
- cotangent: bfloat16 [16, 512, 1024], P(None, 'sp', 'tp'), may hold values from -6 to 6
Outputs:
- grad_queries: bfloat16 [16, 8, 512, 64], P(None, 'tp', 'sp')
- grad_keys: bfloat16 [16, 8, 512, 64], P(None, 'tp', 'sp')
- grad_forward: float32 [16, 8, 512, 64], P(None, 'tp', 'sp')
- grad_backward: float32 [16, 8, 512, 64], P(None, 'tp', 'sp')
- grad_hidden: bfloat16 [16, 512, 1024], P(None, 'sp', 'tp')
- grad_weight: float32 [1024, 1024], P('sp', 'tp')
All inputs are finite; a program needn't handle non-finite values.
Results may differ from a plain program's by a relative error of at most 0.015.
Values may be sent and summed in bfloat16 or wider, within the bound.
A program may use at most 128 MiB of HBM per device.

v0:
```python
import jax
import jax.numpy as jnp
from jax import lax
from jax.sharding import PartitionSpec as P

EXACT_DOTS = lax.Precision.HIGHEST


def carried_in(value, axis, join, neutral, backward):
    count, mine = lax.axis_size(axis), lax.axis_index(axis)
    pieces = jax.tree.map(lambda part: lax.all_gather(part, axis), value)
    if backward:
        pieces = jax.tree.map(lambda part: part[::-1], pieces)
        mine = count - 1 - mine
    running = jax.tree.map(
        lambda part, zero: jnp.full_like(part, 0) + jnp.asarray(zero, part.dtype), value, neutral
    )

    def lap(position, running):
        longer = join(running, jax.tree.map(lambda part: part[position], pieces))
        return jax.tree.map(lambda new, old: jnp.where(position < mine, new, old), longer, running)

    return lax.fori_loop(0, count - 1, lap, running)


def flip_tokens(tensor, axis_number):
    return jnp.flip(tensor, axis=axis_number)


def elements(query_heads, key_heads, value_heads, decay_heads, seed_heads):
    cumulative = jnp.cumsum(decay_heads, axis=2)
    final_sum = cumulative[:, :, -1, :]
    to_end = jnp.exp(final_sum[:, :, None, :] - cumulative)
    factor = jnp.exp(final_sum)
    state_part = jnp.einsum(
        "bhjd,bhje->bhde", key_heads * to_end, value_heads, precision=EXACT_DOTS
    )
    grad_part = jnp.einsum(
        "bhcd,bhce->bhde", query_heads * jnp.exp(cumulative), seed_heads, precision=EXACT_DOTS
    )
    return ((factor, state_part), (factor, grad_part))


def compose(earlier, later):
    return (earlier[0] * later[0], later[0][..., None] * earlier[1] + later[1])


def neutral(element):
    return (jnp.ones_like(element[0]), jnp.zeros_like(element[1]))


def paired(first, second):
    return (jnp.stack([first[0], second[0]]), jnp.stack([first[1], second[1]]))


def block_grads(query_seq, key_seq, value_seq, decay_seq, seed_seq, state_in, grad_in):
    length = query_seq.shape[1]
    seed_real = seed_seq.astype(jnp.float32)
    value_real = value_seq.astype(jnp.float32)
    cumulative = jnp.cumsum(decay_seq, axis=1)
    final_sum = cumulative[:, -1, :]
    growth = jnp.exp(cumulative)
    shrink = jnp.exp(-cumulative)
    to_end = jnp.exp(final_sum[:, None, :] - cumulative)
    query_hat = (query_seq * growth).astype(jnp.bfloat16)
    key_hat = (key_seq * shrink).astype(jnp.bfloat16)
    below_mask = jnp.tril(jnp.ones((length, length), dtype=bool))[None]
    scores = jnp.where(
        below_mask,
        jnp.einsum("hid,hjd->hij", query_hat, key_hat, preferred_element_type=jnp.float32),
        0.0,
    ).astype(jnp.bfloat16)
    seed_scores = jnp.where(
        below_mask,
        jnp.einsum("hie,hje->hij", seed_seq, value_seq, preferred_element_type=jnp.float32),
        0.0,
    ).astype(jnp.bfloat16)
    grad_query = growth * (
        jnp.einsum("hij,hjd->hid", seed_scores, key_hat, preferred_element_type=jnp.float32)
        + jnp.einsum("hce,hde->hcd", seed_real, state_in, precision=EXACT_DOTS)
    )
    grad_key = shrink * jnp.einsum(
        "hij,hid->hjd", seed_scores, query_hat, preferred_element_type=jnp.float32
    )
    grad_key = grad_key + to_end * jnp.einsum(
        "hde,hje->hjd", grad_in, value_real, precision=EXACT_DOTS
    )
    grad_value = jnp.einsum("hij,hie->hje", scores, seed_seq, preferred_element_type=jnp.float32)
    grad_value = grad_value + jnp.einsum(
        "hjd,hde->hje", key_seq * to_end, grad_in, precision=EXACT_DOTS
    )
    grad_cumul = query_seq * grad_query - key_seq * grad_key
    return (grad_query, grad_key, grad_value, grad_cumul)


def shards(hidden, value_weight, queries, key_vectors, forward_decay, backward_decay, cotangent):
    batch_size, length, model_width = hidden.shape
    head_count = queries.shape[1]
    value_width = value_weight.shape[1] // head_count
    hidden_rows = hidden.reshape(batch_size * length, model_width)
    values_flat = jnp.dot(hidden_rows, value_weight, preferred_element_type=jnp.float32).astype(
        jnp.bfloat16
    )

    def to_heads(tensor):
        return tensor.reshape(batch_size, length, head_count, value_width).transpose(0, 2, 1, 3)

    value_narrow = to_heads(values_flat)
    seed_narrow = to_heads(cotangent)
    value_heads = value_narrow.astype(jnp.float32)
    seed_heads = seed_narrow.astype(jnp.float32)
    query_heads = queries.astype(jnp.float32)
    key_heads = key_vectors.astype(jnp.float32)
    ahead_state, ahead_grad = elements(
        query_heads, key_heads, value_heads, forward_decay, seed_heads
    )
    behind_state, behind_grad = elements(
        flip_tokens(query_heads, 2),
        flip_tokens(key_heads, 2),
        flip_tokens(value_heads, 2),
        flip_tokens(backward_decay, 2),
        flip_tokens(seed_heads, 2),
    )
    lower_pair = paired(ahead_state, behind_grad)
    upper_pair = paired(behind_state, ahead_grad)
    from_lower = carried_in(lower_pair, "sp", compose, neutral(lower_pair), False)[1]
    from_higher = carried_in(upper_pair, "sp", compose, neutral(upper_pair), True)[1]
    state_left, grad_left = (from_lower[0], from_lower[1])
    state_right, grad_right = (from_higher[0], from_higher[1])

    def per_sequence(inputs):
        (
            query_seq,
            key_seq,
            value_seq,
            ahead_decay,
            behind_decay,
            seed_seq,
            left_state,
            right_grad,
            right_state,
            left_grad,
        ) = inputs
        ahead = block_grads(
            query_seq, key_seq, value_seq, ahead_decay, seed_seq, left_state, right_grad
        )
        behind = block_grads(
            flip_tokens(query_seq, 1),
            flip_tokens(key_seq, 1),
            flip_tokens(value_seq, 1),
            flip_tokens(behind_decay, 1),
            flip_tokens(seed_seq, 1),
            right_state,
            left_grad,
        )
        return (
            ahead[0] + flip_tokens(behind[0], 1),
            ahead[1] + flip_tokens(behind[1], 1),
            ahead[2] + flip_tokens(behind[2], 1),
            ahead[3],
            flip_tokens(behind[3], 1),
        )

    grad_query, grad_key, grad_value, cumul_ahead, cumul_behind = lax.map(
        per_sequence,
        (
            query_heads,
            key_heads,
            value_narrow,
            forward_decay,
            backward_decay,
            seed_narrow,
            state_left,
            grad_right,
            state_right,
            grad_left,
        ),
    )
    totals = jnp.stack([jnp.sum(cumul_ahead, axis=2), jnp.sum(cumul_behind, axis=2)])
    before = carried_in(
        totals, "sp", lambda earlier, later: earlier + later, jnp.zeros_like(totals), False
    )
    grad_forward = -(before[0][:, :, None, :] + jnp.cumsum(cumul_ahead, axis=2) - cumul_ahead)
    grad_backward = before[1][:, :, None, :] + jnp.cumsum(cumul_behind, axis=2)
    value_rows = (
        grad_value.transpose(0, 2, 1, 3)
        .reshape(batch_size * length, head_count * value_width)
        .astype(jnp.bfloat16)
    )

    def weight_term(row_count):
        columns = lax.slice_in_dim(hidden_rows, 0, row_count, axis=1)
        return lax.dot_general(
            columns, value_rows, (((0,), (0,)), ((), ())), preferred_element_type=jnp.float32
        )

    grad_weight = lax.psum_scatter(
        weight_term(model_width // lax.axis_size("sp") * lax.axis_size("sp")),
        "sp",
        scatter_dimension=0,
        tiled=True,
    )
    input_terms = lax.dot_general(
        value_rows, value_weight, (((1,), (1,)), ((), ())), preferred_element_type=jnp.float32
    ).reshape(batch_size, length, model_width)
    grad_hidden = (
        lax.psum_scatter(input_terms.astype(jnp.bfloat16), "tp", scatter_dimension=2, tiled=True)
        .astype(jnp.float32)
        .astype(jnp.bfloat16)
    )
    return (
        grad_query.astype(jnp.bfloat16),
        grad_key.astype(jnp.bfloat16),
        grad_forward,
        grad_backward,
        grad_hidden,
        grad_weight,
    )


def solution(mesh):
    placed = (
        P(None, "sp", None),
        P(None, "tp"),
        P(None, "tp", "sp", None),
        P(None, "tp", "sp", None),
        P(None, "tp", "sp", None),
        P(None, "tp", "sp", None),
        P(None, "sp", "tp"),
    )
    return jax.shard_map(
        shards,
        mesh=mesh,
        in_specs=placed,
        out_specs=(
            P(None, "tp", "sp", None),
            P(None, "tp", "sp", None),
            P(None, "tp", "sp", None),
            P(None, "tp", "sp", None),
            P(None, "sp", "tp"),
            P("sp", "tp"),
        ),
        check_vma=False,
    )
```

profile of v0, /device:TPU:0, one launch (start us, length us, event | category | flops | bytes accessed | tf_op | source)
XLA Modules:
  0.0 878.1 jit_solution(13302334434391016829)
XLA Ops:
  7.2 1.4 rev.53
  8.7 1.6 fusion.51
  10.2 1.6 fusion.53
  12.7 1.3 fusion.65
  14.1 2.1 rev.58
  17.0 3.0 copy_convert_fusion
  20.0 2.1 exponential_multiply_fusion
  22.1 1.2 reshape.60
  23.3 3.3 exponential_multiply_fusion.1
  26.6 2.3 convolution_bitcast_fusion.1
  28.9 1.4 convolution_bitcast_fusion.3
  30.3 1.5 pad_maximum_fusion.1
  32.1 1.4 bitcast_convert_fusion
  33.5 2.6 rev.55
  36.0 2.8 convolution_bitcast_fusion.4
  38.8 2.3 convolution_bitcast_fusion.2
  41.2 1.5 pad_maximum_fusion
  43.7 33.9 %all-gather.2 = f32[16,16,2,64]{3,1,2,0:T(8,128)S(1)} all-gather(f32[2,16,2,64]{3,1,2,0:T(8,128)S(1)} %get-tuple-element.619), channel_id=4, replica_groups=mesh['sp'=8,'tp'=4] {'sp'}, dimensions={0}, use_global_device_ids=true | all-gather | bytes 147456 | tf_op jit(solution)/shard_map/all_gather | solution.py:11
  77.8 31.6 %all-gather = f32[16,16,2,64]{3,1,2,0:T(8,128)S(1)} all-gather(f32[2,16,2,64]{3,1,2,0:T(8,128)S(1)} %get-tuple-element.620), channel_id=2, replica_groups=mesh['sp'=8,'tp'=4] {'sp'}, dimensions={0}, use_global_device_ids=true | all-gather | bytes 147456 | tf_op jit(solution)/shard_map/all_gather | solution.py:11
  109.4 156.9 %all-gather.10.cloned.1.call-done = f32[16,16,2,64,128]{4,3,2,1,0:T(8,128)} async-done(((f32[2,16,2,64,128]{4,3,2,1,0:T(8,128)}), f32[16,16,2,64,128]{4,3,2,1,0:T(8,128)}) %all-gather.10.cloned.1.call-update) | async-done | bytes 16777232 | tf_op jit(solution)/shard_map/all_gather | solution.py:11
  266.3 11.8 %rev.59 = f32[8,2,16,2,64,128]{5,4,3,2,1,0:T(8,128)} reverse(f32[8,2,16,2,64,128]{5,4,3,2,1,0:T(8,128)} %bitcast.259), dimensions={0} | reverse | bytes 33554432 | tf_op jit(solution)/shard_map/rev | solution.py:13
  278.1 24.2 %while.62 = (s32[]{:T(128)}, f32[2,16,2,64,128]{4,3,2,1,0:T(8,128)}, s32[]{:T(128)}, f32[8,2,16,2,64]{4,3,2,1,0:T(2,128)S(1)}, f32[8,2,16,2,64,128]{5,4,3,2,1,0:T(8,128)}, /*index=5*/s32[]{:T(128)}, s32[]{:T(128)}) while((s32[]{:T(128)}, f32[2,16,2,64,128]{4,3,2,1,0:T(8,128)}, s32[]{:T(128)}, f32[8,2,16,2,64]{4,3,2,1,0:T(2,128)S(1)}, ...), condition=%wide.region_5.6_spmd.clone, body=%wide.region_4.5_spmd.clone.sunk | while | flops 2097156 | bytes 6340713 | solution.py:23
  278.1 3.0 fusion.163
  281.1 3.5 fusion.163
  284.6 3.5 fusion.163
  288.1 3.5 fusion.163
  291.7 3.5 fusion.163
  295.2 3.5 fusion.163
  298.7 3.5 fusion.163
  302.2 3.1 slice_bitcast_fusion.1
  305.4 188.1 %all-gather.8.cloned.1.call-done = f32[16,16,2,64,128]{4,3,2,1,0:T(8,128)} async-done(((f32[2,16,2,64,128]{4,3,2,1,0:T(8,128)}), f32[16,16,2,64,128]{4,3,2,1,0:T(8,128)}) %all-gather.8.cloned.1.call-update) | async-done | bytes 16777232 | tf_op jit(solution)/shard_map/all_gather | solution.py:11
  493.5 24.9 %while.61 = (s32[]{:T(128)}, f32[2,16,2,64,128]{4,3,2,1,0:T(8,128)}, s32[]{:T(128)}, f32[8,2,16,2,64]{4,2,3,1,0:T(8,128)S(1)}, f32[8,2,16,2,64,128]{5,4,3,2,1,0:T(8,128)}, /*index=5*/s32[]{:T(128)}, s32[]{:T(128)}) while((s32[]{:T(128)}, f32[2,16,2,64,128]{4,3,2,1,0:T(8,128)}, s32[]{:T(128)}, f32[8,2,16,2,64]{4,2,3,1,0:T(8,128)S(1)}, ...), condition=%wide.region_3.4_spmd.clone, body=%wide.region_2.3_spmd.clone.sunk | while | flops 2097156 | bytes 6373481 | solution.py:23
  493.5 3.1 fusion.162
  496.6 3.6 fusion.162
  500.2 3.6 fusion.162
  503.9 3.6 fusion.162
  507.5 3.6 fusion.162
  511.1 3.6 fusion.162
  514.8 3.6 fusion.162
  518.4 3.2 slice_bitcast_fusion
  521.5 251.1 %while.60 = (s32[]{:T(128)}, bf16[16,2,64,64]{3,2,1,0:T(8,128)(2,1)}, bf16[16,2,64,64]{3,2,1,0:T(8,128)(2,1)}, bf16[16,2,64,128]{3,2,1,0:T(8,128)(2,1)S(1)}, f32...) while((s32[]{:T(128)}, ...), condition=%wide.region_9.10_spmd, body=%wide.region_6.9_spmd.sunk | while | flops 91664384 | bytes 4421317 | solution.py:164
  526.5 1.1 constant_dynamic-slice_fusion.8
  542.2 1.1 constant_dynamic-slice_fusion.8
  557.9 1.1 constant_dynamic-slice_fusion.8
  573.6 1.1 constant_dynamic-slice_fusion.8
  589.3 1.1 constant_dynamic-slice_fusion.8
  605.0 1.1 constant_dynamic-slice_fusion.8
  620.7 1.1 constant_dynamic-slice_fusion.8
  636.4 1.1 constant_dynamic-slice_fusion.8
  652.1 1.1 constant_dynamic-slice_fusion.8
  714.8 1.1 constant_dynamic-slice_fusion.8
  730.5 1.1 constant_dynamic-slice_fusion.8
  746.2 1.1 constant_dynamic-slice_fusion.8
  761.9 1.1 constant_dynamic-slice_fusion.8
  773.2 1.7 convolution_bitcast_fusion
  775.0 3.4 convolution_convert_fusion
  778.5 1.3 reduce_sum.19
  779.9 31.3 %all-gather.4 = f32[16,16,2,64]{3,1,2,0:T(8,128)S(1)} all-gather(f32[2,16,2,64]{3,1,2,0:T(8,128)S(1)} %copy.119), channel_id=6, replica_groups=mesh['sp'=8,'tp'=4] {'sp'}, dimensions={0}, use_global_device_ids=true | all-gather | bytes 147456 | tf_op jit(solution)/shard_map/all_gather | solution.py:11
  811.7 1.8 broadcast_add_fusion
  813.5 1.6 copy.129
  815.8 1.6 copy.128
  817.4 21.2 %reduce-scatter.5.cloned.1.call-done = f32[128,256]{0,1:T(8,128)} async-done(((f32[1024,256]{0,1:T(8,128)}), f32[128,256]{0,1:T(8,128)}) %reduce-scatter.5.cloned.1.call-update) | async-done | bytes 131088 | tf_op jit(solution)/shard_map/reduce_scatter | solution.py:197
  838.6 1.7 copy.130
  840.3 31.3 %reduce-scatter.3.cloned.1.call-done = bf16[16,64,256]{2,1,0:T(8,128)(2,1)} async-done(((bf16[16,64,1024]{2,1,0:T(8,128)(2,1)}), bf16[16,64,256]{2,1,0:T(8,128)(2,1)}) %reduce-scatter.3.cloned.1.call-update) | async-done | bytes 524304 | tf_op jit(solution)/shard_map/reduce_scatter | solution.py:207
  (686 shorter events, 240.9 us)
Async XLA Ops:
  7.2 4.7 copy-start
  7.2 259.1 %all-gather.10.cloned.1.call-start = ((), (), s32[]{:S(2)}) async-start(), calls=%async_computation.5 | async-start | bytes 18874368 | tf_op jit(solution)/shard_map/all_gather | solution.py:11
  8.6 1.6 copy-start.10
  8.7 3.2 copy-start.11
  12.7 4.3 copy-start.8
  16.1 3.9 copy-start.2
  16.1 3.9 copy-start.9
  23.3 3.3 copy-start.4
  26.6 2.3 copy-start.6
  31.8 461.6 %all-gather.8.cloned.1.call-start = ((), (), s32[]{:S(2)}) async-start(), calls=%async_computation.4 | async-start | bytes 18874368 | tf_op jit(solution)/shard_map/all_gather | solution.py:11
  36.0 2.8 copy-start.3
  36.0 2.8 copy-start.5
  42.7 795.9 %reduce-scatter.5.cloned.1.call-start = ((), (), s32[]{:S(2)}) async-start(), calls=%async_computation.3 | async-start | bytes 1179648 | tf_op jit(solution)/shard_map/reduce_scatter | solution.py:197
  772.6 2.3 copy-start.7
  774.9 3.5 copy-start.1
  775.0 96.6 %reduce-scatter.3.cloned.1.call-start = ((), (), s32[]{:S(2)}) async-start(), calls=%async_computation.2 | async-start | bytes 2621440 | tf_op jit(solution)/shard_map/reduce_scatter | solution.py:207
Sparse Core Ops, SparseCore 0:
  31.9 234.2 all-gather.9
  268.4 225.0 all-gather.7
  775.1 63.4 reduce-scatter.4
  841.5 29.9 reduce-scatter.2
where the time goes:
time: 888 us; the launch traced here: 878 us
  waiting for transfers between devices  398 us (45%)
  matrix products  140 us (16%)
  local copies, waits for them, and re-layouts  122 us (14%)
  other arithmetic  105 us (12%)
  blocking collectives  96.8 us (11%)
  between operations  14 us (2%)
    all_gather x2, waiting for transfers between devices, carried_in(): pieces = jax.tree.map(lambda part: lax.all_gather(part, axis), value)  345 us
    all_gather x3, blocking collectives, carried_in(): pieces = jax.tree.map(lambda part: lax.all_gather(part, axis), value)  96.8 us
    squeeze x64, local copies, waits for them, and re-layouts, shards(): lax.map(per_sequence, (query_heads, key_heads, value_narrow, forward_deca...  51.6 us
    select_n x21, other arithmetic, lap(): jnp.where(position < mine, new, old)  49 us
    dynamic_slice x32, local copies, waits for them, and re-layouts, shards(): lax.map(per_sequence, (query_heads, key_heads, value_narrow, forward_deca...  35.1 us
    dot_general x32, matrix products, block_grads(): jnp.einsum('hjd,hde->hje', key_seq * to_end, grad_in, precision=EXACT_DOTS)  34.1 us
    dot_general x32, matrix products, block_grads(): jnp.einsum('hde,hje->hjd', grad_in, value_real, precision=EXACT_DOTS)  33.1 us
    dot_general x32, matrix products, block_grads(): jnp.einsum('hce,hde->hcd', seed_real, state_in, precision=EXACT_DOTS)  32.8 us
  transfers between devices with their start and end apart: 4, of which 4 were waited for; matrix products, arithmetic and copies ran while one was open for 7% of the time, Pallas kernels for 0%

commit v1 on v0

v1 whole, which is shorter than its diff:
```python
import functools

import jax
import jax.numpy as jnp
from jax import lax
from jax.experimental import pallas as pl
from jax.experimental.pallas import tpu as pltpu
from jax.sharding import PartitionSpec as P

F32, BF16 = jnp.float32, jnp.bfloat16
MESH = pl.DeviceIdType.MESH
LAG = 1


def dot(a, b, ca=1, cb=0):
    return lax.dot_general(a, b, (((ca,), (cb,)), ((), ())), preferred_element_type=F32)


def split(x):
    high = x.astype(BF16)
    return high, (x - high.astype(F32)).astype(BF16)


def plan(sp, batch, heads):
    outer = 4 if sp % 4 == 0 and batch % (sp // 4) == 0 else sp
    inner = sp // outer
    own = batch // inner
    return outer, inner, own, own * heads


def kernel(dims, hid, wgt, qry, key, fdec, bdec, cot,
           o_q, o_k, o_f, o_b, o_h, o_w,
           val, cum, intra_q, intra_k, intra_v,
           a_out, a_in, b_out, b_in, c_out, c_in, d_all, w_in, g_out, g_in,
           a_ss, a_rs, b_ss, b_rs, c_ss, c_rs, d_ss, d_rs, w_ss, w_rs, g_ss, g_rs):
    sp, tp, batch, heads, length, dk, dv, width = dims
    outer, inner, own, units = plan(sp, batch, heads)
    pack = 2 * dk
    feat = width // tp
    rows_sp = width // sp
    group = d_group(own)
    spi, tpi = lax.axis_index("sp"), lax.axis_index("tp")
    z, y = spi // inner, lax.rem(spi, inner)

    barrier = pltpu.get_barrier_semaphore()
    for r in range(1, sp):
        pl.semaphore_signal(barrier, inc=1, device_id={"sp": lax.rem(spi + r, sp)}, device_id_type=MESH)
    for r in range(1, tp):
        pl.semaphore_signal(barrier, inc=1, device_id={"tp": lax.rem(tpi + r, tp)}, device_id_type=MESH)
    pl.semaphore_wait(barrier, sp + tp - 2)

    def remote(src, dst, ss, rs, **where):
        return pltpu.make_async_remote_copy(src_ref=src, dst_ref=dst, send_sem=ss, recv_sem=rs,
                                            device_id=where, device_id_type=MESH)

    def w_copy(r):
        to = lax.rem(tpi + r, tp)
        return remote(wgt.at[pl.ds(pl.multiple_of(to * feat, feat), feat), :], w_in.at[r],
                      w_ss.at[r - 1], w_rs.at[r - 1], tp=to)

    def member(r):
        return lax.rem(y + r, inner)

    def a_copy(side, r, u):
        return remote(a_out.at[side, r - 1, u], a_in.at[side, r, u], a_ss.at[side, r - 1, u],
                      a_rs.at[side, r - 1, u], sp=z * inner + member(r))

    def b_copy(side, u):
        to = z + 1 if side == 0 else z - 1
        to = jnp.clip(to, 0, outer - 1)
        return remote(b_out.at[side, u], b_in.at[side, u], b_ss.at[side, u], b_rs.at[side, u],
                      sp=to * inner + y)

    def c_copy(side, r, u):
        return remote(c_out.at[side, r, u], c_in.at[side, r, u], c_ss.at[side, r - 1, u],
                      c_rs.at[side, r - 1, u], sp=z * inner + member(r))

    messages = own // group

    def d_copy(t, r, h, m):
        owner = lax.rem(y - r + inner, inner)
        first = pl.multiple_of((owner * own + m * group) * length, length)
        return remote(d_all.at[0, h, pl.ds(first, group * length), :],
                      d_all.at[t, h, pl.ds(first, group * length), :],
                      d_ss.at[t - 1, r, h, m], d_rs.at[t - 1, r, h, m], tp=lax.rem(tpi + t, tp))

    def d_wait(t, r, h, m):
        d_copy(t, r, h, m).wait_recv()

    def g_copy(r, h):
        to = lax.rem(spi + r, sp)
        return remote(g_out.at[h, to], g_in.at[h, r], g_ss.at[h, r - 1], g_rs.at[h, r - 1], sp=to)

    for r in range(1, tp):
        w_copy(r).start()
    w_in[0] = wgt[pl.ds(pl.multiple_of(tpi * feat, feat), feat), :]

    chunk = 4 * length
    total = batch * length

    def values(i, _):
        at = pl.ds(pl.multiple_of(i * chunk, chunk), chunk)
        val[at, :] = dot(hid[at, :], wgt[...]).astype(BF16)
        return 0

    lax.fori_loop(0, total // chunk, values, 0)

    row = lax.broadcasted_iota(jnp.int32, (length, length), 0)
    col = lax.broadcasted_iota(jnp.int32, (length, length), 1)
    lower, upper = row >= col, row <= col
    ones_lower, ones_upper = jnp.where(lower, 1.0, 0.0), jnp.where(upper, 1.0, 0.0)
    sums = jnp.concatenate([ones_lower, ones_upper], 0).astype(BF16)
    strict = jnp.concatenate([jnp.where(row > col, 1.0, 0.0), jnp.where(row < col, 1.0, 0.0)], 0).astype(BF16)
    left = lax.broadcasted_iota(jnp.int32, (length, pack), 1) < dk
    tail_row = lax.broadcasted_iota(jnp.int32, (16, pack), 0)
    ones_tail = jnp.ones((16, dv), BF16)
    ones_dv = jnp.ones((16, dv), BF16)

    def both(matrix, x):
        high, low = split(x)
        out = dot(matrix, high) + dot(matrix, low)
        return jnp.where(left, out[:length], out[length:])

    def head_cols(ref, b, h):
        at = pl.ds(pl.multiple_of(b * length, length), length)
        return ref[at, pl.ds(pl.multiple_of(h * dv, dv), dv)]

    def twice(ref, b, h):
        x = ref[b, h].astype(F32)
        return jnp.concatenate([x, x], 1)

    def parts(b, h):
        c = both(sums, jnp.concatenate([fdec[b, h], bdec[b, h]], 1))
        cum[b, h] = c
        end = jnp.where(left[:1], c[length - 1:length], c[0:1])
        grow = (twice(qry, b, h) * jnp.exp(c)).astype(BF16)
        decay_key = (twice(key, b, h) * jnp.exp(end - c)).astype(BF16)
        state = dot(decay_key, head_cols(val, b, h), 0, 0)
        grad = dot(grow, head_cols(cot, b, h), 0, 0)
        high = end.astype(BF16).astype(F32)
        tail = jnp.where(tail_row == 0, high, jnp.where(tail_row == 1, end - high, 0.0))
        low = jnp.concatenate([state[:dk], grad[dk:], tail], 0).astype(BF16)
        up = jnp.concatenate([grad[:dk], state[dk:], tail], 0).astype(BF16)
        return low, up

    def phase_one(u, _):
        h, step = u // own, lax.rem(u, own)
        made = [parts(member(r) * own + step, h) for r in range(inner)]
        for r in range(1, inner):
            for side in range(2):
                a_out[side, r - 1, u] = made[r][side]
        for side in range(2):
            a_in[side, 0, u] = made[0][side]
        for r in range(1, inner):
            for side in range(2):
                a_copy(side, r, u).start()
        return 0

    lax.fori_loop(0, units, phase_one, 0)

    def intra(b, h):
        c = cum[b, h]
        q_hat = (twice(qry, b, h) * jnp.exp(c)).astype(BF16)
        k_hat = (twice(key, b, h) * jnp.exp(-c)).astype(BF16)
        v, seed = head_cols(val, b, h), head_cols(cot, b, h)
        seed_scores = dot(seed, v, 1, 1)
        zero = jnp.zeros_like(q_hat)
        q_left, q_right = jnp.where(left, q_hat, zero), jnp.where(left, zero, q_hat)
        k_left, k_right = jnp.where(left, k_hat, zero), jnp.where(left, zero, k_hat)
        score = (jnp.where(lower, dot(q_left, k_hat, 1, 1), 0.0)
                 + jnp.where(upper, dot(q_right, k_hat, 1, 1), 0.0)).astype(BF16)
        seed_low = jnp.where(lower, seed_scores, 0.0).astype(BF16)
        seed_up = jnp.where(upper, seed_scores, 0.0).astype(BF16)
        intra_q[b, h] = dot(seed_low, k_left) + dot(seed_up, k_right)
        intra_k[b, h] = dot(seed_low, q_left, 0, 0) + dot(seed_up, q_right, 0, 0)
        intra_v[b, h] = dot(score, seed, 0, 0)

    def combine(side, u):
        @pl.when((z > 0) if side == 0 else (z < outer - 1))
        def _():
            b_copy(side, u).wait_recv()

        first = (z == 0) if side == 0 else (z == outer - 1)

        @pl.when(first)
        def _():
            b_in[side, u] = jnp.zeros((pack, dv), BF16)

        for r in range(1, inner):
            a_copy(side, r, u).wait_recv()
        running = b_in[side, u].astype(F32)
        order = range(inner) if side == 0 else range(inner - 1, -1, -1)
        for person in order:
            r = lax.rem(person - y + inner, inner)
            source = lax.rem(y - person + inner, inner)
            c_out[side, r, u] = running.astype(BF16)
            message = a_in[side, source, u]
            factor = jnp.exp(dot(message[pack:], ones_tail, 0, 0))
            running = factor * running + message[:pack].astype(F32)
        b_out[side, u] = running.astype(BF16)

        @pl.when((z < outer - 1) if side == 0 else (z > 0))
        def _():
            b_copy(side, u).start()

        c_in[side, 0, u] = c_out[side, 0, u]
        for r in range(1, inner):
            c_copy(side, r, u).start()

    def finish(r, u, h, step):
        b = lax.rem(y - r + inner, inner) * own + step
        low, up = c_in[0, r, u], c_in[1, r, u]
        state = jnp.concatenate([low[:dk], up[dk:]], 0)
        grad = jnp.concatenate([up[:dk], low[dk:]], 0)
        c = cum[b, h]
        end = jnp.where(left[:1], c[length - 1:length], c[0:1])
        grow, shrink, to_end = jnp.exp(c), jnp.exp(-c), jnp.exp(end - c)
        q, k = twice(qry, b, h), twice(key, b, h)
        v, seed = head_cols(val, b, h), head_cols(cot, b, h)
        cross = dot(seed, state, 1, 1)
        dq = grow * (intra_q[b, h] + cross)
        dk_ = shrink * intra_k[b, h] + to_end * dot(v, grad, 1, 1)
        dv_ = intra_v[b, h] + dot((k * to_end).astype(BF16), grad)
        g = q * dq - k * dk_
        pair = (state.astype(F32) * grad.astype(F32)).astype(BF16)
        start = (jnp.sum(q * grow * cross, axis=0, keepdims=True)
                 + jnp.exp(end) * dot(ones_dv, pair, 1, 1)[:1])
        decay_grad = start - both(strict, g)
        o_q[b, h] = (dq[:, :dk] + dq[:, dk:]).astype(BF16)
        o_k[b, h] = (dk_[:, :dk] + dk_[:, dk:]).astype(BF16)
        o_f[b, h] = decay_grad[:, :dk]
        o_b[b, h] = decay_grad[:, dk:]
        d_all[0, h, pl.ds(pl.multiple_of(b * length, length), length), :] = dv_.astype(BF16)

    def weight_term(h):
        full = dot(d_all[0, h], hid[...], 0, 0)
        for p in range(sp):
            g_out[h, p] = full[:, p * rows_sp:(p + 1) * rows_sp].astype(BF16)
        for r in range(1, sp):
            g_copy(r, h).start()

    reach = (outer - 1) * LAG
    delay = reach + 1

    def phase_two(s, _):
        @pl.when(s < units)
        def _():
            h, step = s // own, lax.rem(s, own)
            for r in range(inner):
                intra(r * own + step, h)

        for side in range(2):
            at = s - (z if side == 0 else outer - 1 - z) * LAG

            @pl.when((at >= 0) & (at < units))
            def _():
                combine(side, at)

        last = s - delay

        @pl.when(last >= 0)
        def _():
            h, step = last // own, lax.rem(last, own)
            for side in range(2):
                for r in range(1, inner):
                    c_copy(side, r, last).wait_recv()
            for r in range(inner):
                finish(r, last, h, step)

            @pl.when(lax.rem(step + 1, group) == 0)
            def _():
                m = step // group
                for r in range(inner):
                    for t in range(1, tp):
                        d_copy(t, r, h, m).start()

            @pl.when(step == own - 1)
            def _():
                weight_term(h)
        return 0

    lax.fori_loop(0, units + delay, phase_two, 0)

    for t in range(1, tp):
        w_copy(t).wait_recv()
        for r in range(inner):
            for h in range(heads):
                for m in range(messages):
                    d_wait(t, r, h, m)

    def features(i, _):
        at = pl.ds(pl.multiple_of(i * chunk, chunk), chunk)
        acc = jnp.zeros((chunk, feat), F32)
        for t in range(tp):
            for h in range(heads):
                acc = acc + dot(d_all[t, h, at, :], w_in[t, :, h * dv:(h + 1) * dv], 1, 1)
        o_h[at, :] = acc.astype(BF16)
        return 0

    lax.fori_loop(0, total // chunk, features, 0)

    for h in range(heads):
        acc = g_out[h, spi].astype(F32)
        for r in range(1, sp):
            g_copy(r, h).wait_recv()
            acc = acc + g_in[h, r].astype(F32)
        o_w[:, h * dv:(h + 1) * dv] = acc.T

    for r in range(1, tp):
        w_copy(r).wait_send()
    for h in range(heads):
        for r in range(1, sp):
            g_copy(r, h).wait_send()
        for m in range(messages):
            for t in range(1, tp):
                for r in range(inner):
                    d_copy(t, r, h, m).wait_send()

    def drain(u, _):
        for side in range(2):
            for r in range(1, inner):
                a_copy(side, r, u).wait_send()
                c_copy(side, r, u).wait_send()

            @pl.when((z < outer - 1) if side == 0 else (z > 0))
            def _():
                b_copy(side, u).wait_send()
        return 0

    lax.fori_loop(0, units, drain, 0)


def d_group(own):
    return 4 if own % 4 == 0 else 1


def shards(sp, tp, hidden, value_weight, queries, key_vectors, forward_decay, backward_decay, cotangent):
    batch, length, width = hidden.shape
    heads, dk = queries.shape[1], queries.shape[3]
    cols = value_weight.shape[1]
    dv = cols // heads
    outer, inner, own, units = plan(sp, batch, heads)
    pack, rows, feat, rows_sp = 2 * dk, batch * length, width // tp, width // sp
    group = d_group(own)
    dims = (sp, tp, batch, heads, length, dk, dv, width)
    vmem, dma = pltpu.VMEM, pltpu.SemaphoreType.DMA
    peers = max(inner - 1, 1)
    scratch = [
        vmem((rows, cols), BF16),
        vmem((batch, heads, length, pack), F32),
        vmem((batch, heads, length, pack), F32),
        vmem((batch, heads, length, pack), F32),
        vmem((batch, heads, length, dv), F32),
        vmem((2, peers, units, pack + 16, dv), BF16),
        vmem((2, inner, units, pack + 16, dv), BF16),
        vmem((2, units, pack, dv), BF16),
        vmem((2, units, pack, dv), BF16),
        vmem((2, inner, units, pack, dv), BF16),
        vmem((2, inner, units, pack, dv), BF16),
        vmem((tp, heads, rows, dv), BF16),
        vmem((tp, feat, cols), BF16),
        vmem((heads, sp, dv, rows_sp), BF16),
        vmem((heads, sp, dv, rows_sp), BF16),
        dma((2, peers, units)), dma((2, peers, units)),
        dma((2, units)), dma((2, units)),
        dma((2, peers, units)), dma((2, peers, units)),
        dma((tp - 1, inner, heads, own // group)), dma((tp - 1, inner, heads, own // group)),
        dma((tp - 1,)), dma((tp - 1,)),
        dma((heads, sp - 1)), dma((heads, sp - 1)),
    ]
    whole = pl.BlockSpec(memory_space=vmem)
    outs = pl.pallas_call(
        functools.partial(kernel, dims),
        out_shape=(
            jax.ShapeDtypeStruct(queries.shape, BF16),
            jax.ShapeDtypeStruct(queries.shape, BF16),
            jax.ShapeDtypeStruct(queries.shape, F32),
            jax.ShapeDtypeStruct(queries.shape, F32),
            jax.ShapeDtypeStruct((rows, feat), BF16),
            jax.ShapeDtypeStruct((rows_sp, cols), F32),
        ),
        in_specs=[whole] * 7,
        out_specs=(whole,) * 6,
        scratch_shapes=scratch,
        compiler_params=pltpu.CompilerParams(
            collective_id=0, has_side_effects=True, vmem_limit_bytes=60 * 1024 * 1024
        ),
    )(hidden.reshape(rows, width), value_weight, queries, key_vectors, forward_decay, backward_decay,
      cotangent.reshape(rows, cols))
    return (outs[0], outs[1], outs[2], outs[3], outs[4].reshape(batch, length, feat), outs[5])


def solution(mesh):
    heads = P(None, "tp", "sp", None)
    return jax.shard_map(
        functools.partial(shards, mesh.shape["sp"], mesh.shape["tp"]),
        mesh=mesh,
        in_specs=(P(None, "sp", None), P(None, "tp"), heads, heads, heads, heads, P(None, "sp", "tp")),
        out_specs=(heads, heads, heads, heads, P(None, "sp", "tp"), P("sp", "tp")),
        check_vma=False,
    )
```

time: 888 us -> 108 us (0.12); the launches traced: 878 us -> 108 us
  waiting for transfers between devices: 398 us -> 0 us
  matrix products: 140 us -> 0 us
  local copies, waits for them, and re-layouts: 122 us -> 7.31 us
  other arithmetic: 105 us -> 0 us
  Pallas kernels: 0 us -> 100 us
  blocking collectives: 96.8 us -> 0 us
  between operations: 14 us -> 0.66 us
    all_gather x2 -> x0, waiting for transfers between devices: 345 us -> none  [carried_in(): pieces = jax.tree.map(lambda part: lax.all_gather(part, axis), value)]
    dot_general x231 -> x0, matrix products: 140 us -> none  [the longest x32 34.1 us: block_grads(): jnp.einsum('hjd,hde->hje', key_seq * to_end, grad_in, precision=EXACT_DOTS)]
    pallas_call x0 -> x1, Pallas kernels: none -> 100 us  [shards(): pl.pallas_call(functools.partial(kernel, dims), out_shape=(jax.ShapeDtype...]
    all_gather x3 -> x0, blocking collectives: 96.8 us -> none  [carried_in(): pieces = jax.tree.map(lambda part: lax.all_gather(part, axis), value)]
    squeeze x66 -> x0, local copies, waits for them, and re-layouts: 57.9 us -> none  [the longest x64 51.6 us: shards(): lax.map(per_sequence, (query_heads, key_heads, value_narrow, forward_deca...]
    reduce_scatter x2 -> x0, waiting for transfers between devices: 52.5 us -> none  [the longest x1 31.3 us: shards(): lax.psum_scatter(input_terms.astype(jnp.bfloat16), 'tp', scatter_dimensio...]
    select_n x21 -> x0, other arithmetic: 49 us -> none  [lap(): jnp.where(position < mine, new, old)]
    dynamic_slice x53 -> x0, local copies, waits for them, and re-layouts: 35.3 us -> none  [the longest x32 35.1 us: shards(): lax.map(per_sequence, (query_heads, key_heads, value_narrow, forward_deca...]
  transfers between devices with their start and end apart: 4 -> 0, of which waited for: 4 -> 0; matrix products, arithmetic and copies ran while one was open for 7% -> 0% of each run, Pallas kernels for 0% -> 0%
where the time goes in v1:
time: 108 us
  Pallas kernels  100 us (93%)
  local copies, waits for them, and re-layouts  7.31 us (7%)
    pallas_call x1, Pallas kernels, shards(): pl.pallas_call(functools.partial(kernel, dims), out_shape=(jax.ShapeDtype...  100 us
    unnamed x14, local copies, waits for them, and re-layouts  7.31 us

profile of v1, /device:TPU:0, one launch (start us, length us, event | category | flops | bytes accessed | tf_op | source)
XLA Modules:
  0.0 108.0 jit_solution(336757310683879964)
XLA Ops:
  0.6 100.0 %shard_map.118 = (bf16[16,2,64,64]{3,2,1,0:T(8,128)(2,1)}, bf16[16,2,64,64]{3,2,1,0:T(8,128)(2,1)}, f32[16,2,64,64]{3,2,1,0:T(8,128)}, f32[16,2,64,64]{3,2,1,0:T...) custom-call(bf16[1024,1024]{1,0:T(8,128)(2,1)} %bitcast.3, bf16[1024,256]{1,0:T(8,128)(2,1)} %wgt.1, ...), custom_call_target="tpu_custom_call" | custom-call | tf_op jit(solution)/shard_map/pallas_call | solution.py:372
  100.6 0.0 copy-start.1
  100.6 0.0 copy-start
  100.7 2.0 %copy.19 = bf16[16,2,64,64]{3,2,1,0:T(8,128)(2,1)} copy(bf16[16,2,64,64]{3,2,1,0:T(8,128)(2,1)} %get-tuple-element.24) | data formatting | bytes 524288
  102.7 1.9 %copy.20 = bf16[16,2,64,64]{3,2,1,0:T(8,128)(2,1)} copy(bf16[16,2,64,64]{3,2,1,0:T(8,128)(2,1)} %get-tuple-element.25) | data formatting | bytes 524288
  104.6 0.0 copy-done.1
  104.6 0.0 copy-start.2
  104.6 0.0 copy-start.3
  104.6 1.0 copy.21
  105.5 0.0 copy-done
  105.5 1.0 copy.22
  106.5 0.0 copy-done.2
  106.5 0.8 copy.23
  107.3 0.0 copy-done.3
  107.3 0.7 copy.24
Async XLA Ops:
  100.6 3.9 %copy-start.1 = (f32[16,2,64,64]{3,2,1,0:T(8,128)S(1)}, f32[16,2,64,64]{3,2,1,0:T(8,128)}, u32[]{:S(2)}) copy-start(f32[16,2,64,64]{3,2,1,0:T(8,128)} %get-tuple-element.26) | copy-start | bytes 1572868
  100.6 4.9 %copy-start = (f32[16,2,64,64]{3,2,1,0:T(8,128)S(1)}, f32[16,2,64,64]{3,2,1,0:T(8,128)}, u32[]{:S(2)}) copy-start(f32[16,2,64,64]{3,2,1,0:T(8,128)} %get-tuple-element.27) | copy-start | bytes 1572868
  104.6 1.9 %copy-start.2 = (bf16[1024,256]{1,0:T(8,128)(2,1)S(1)}, bf16[1024,256]{1,0:T(8,128)(2,1)}, u32[]{:S(2)}) copy-start(bf16[1024,256]{1,0:T(8,128)(2,1)} %get-tuple-element.16) | copy-start | bytes 1572868
  104.6 2.7 %copy-start.3 = (f32[128,256]{1,0:T(8,128)S(1)}, f32[128,256]{1,0:T(8,128)}, u32[]{:S(2)}) copy-start(f32[128,256]{1,0:T(8,128)} %get-tuple-element.29) | copy-start | bytes 393220

commit v2 on v1

--- a/solution.py
+++ b/solution.py
@@ -9,7 +9,8 @@
 
 F32, BF16 = jnp.float32, jnp.bfloat16
 MESH = pl.DeviceIdType.MESH
-LAG = 1
+LAG = 2
+EXTRA = 4
 
 
 def dot(a, b, ca=1, cb=0):
@@ -29,7 +30,7 @@
 
 
 def kernel(dims, hid, wgt, qry, key, fdec, bdec, cot,
-           o_q, o_k, o_f, o_b, o_h, o_w,
+           o_qk, o_fb, o_h, o_w,
            val, cum, intra_q, intra_k, intra_v,
            a_out, a_in, b_out, b_in, c_out, c_in, d_all, w_in, g_out, g_in,
            a_ss, a_rs, b_ss, b_rs, c_ss, c_rs, d_ss, d_rs, w_ss, w_rs, g_ss, g_rs):
@@ -103,7 +104,16 @@
         val[at, :] = dot(hid[at, :], wgt[...]).astype(BF16)
         return 0
 
-    lax.fori_loop(0, total // chunk, values, 0)
+    mine = own * length // chunk if own * length % chunk == 0 else 0
+
+    def values_of(r):
+        lax.fori_loop(0, mine, lambda i, _: values(member(r) * mine + i, 0), 0)
+
+    if mine:
+        for r in range(1, inner):
+            values_of(r)
+    else:
+        lax.fori_loop(0, total // chunk, values, 0)
 
     row = lax.broadcasted_iota(jnp.int32, (length, length), 0)
     col = lax.broadcasted_iota(jnp.int32, (length, length), 1)
@@ -143,20 +153,22 @@
         up = jnp.concatenate([grad[:dk], state[dk:], tail], 0).astype(BF16)
         return low, up
 
-    def phase_one(u, _):
-        h, step = u // own, lax.rem(u, own)
-        made = [parts(member(r) * own + step, h) for r in range(inner)]
-        for r in range(1, inner):
+    pair = 2 if units % 2 == 0 else 1
+
+    def phase_one(i, _):
+        todo = [(r, i * pair + n) for n in range(pair) for r in range(1, inner)]
+        made = [parts(member(r) * own + lax.rem(u, own), u // own) for r, u in todo]
+        for (r, u), sides in zip(todo, made):
             for side in range(2):
-                a_out[side, r - 1, u] = made[r][side]
-        for side in range(2):
-            a_in[side, 0, u] = made[0][side]
-        for r in range(1, inner):
+                a_out[side, r - 1, u] = sides[side]
+        for r, u in todo:
             for side in range(2):
                 a_copy(side, r, u).start()
         return 0
 
-    lax.fori_loop(0, units, phase_one, 0)
+    lax.fori_loop(0, units // pair, phase_one, 0)
+    if mine:
+        values_of(0)
 
     def intra(b, h):
         c = cum[b, h]
@@ -226,10 +238,8 @@
         start = (jnp.sum(q * grow * cross, axis=0, keepdims=True)
                  + jnp.exp(end) * dot(ones_dv, pair, 1, 1)[:1])
         decay_grad = start - both(strict, g)
-        o_q[b, h] = (dq[:, :dk] + dq[:, dk:]).astype(BF16)
-        o_k[b, h] = (dk_[:, :dk] + dk_[:, dk:]).astype(BF16)
-        o_f[b, h] = decay_grad[:, :dk]
-        o_b[b, h] = decay_grad[:, dk:]
+        o_qk[b, h] = jnp.concatenate([dq[:, :dk] + dq[:, dk:], dk_[:, :dk] + dk_[:, dk:]], 1).astype(BF16)
+        o_fb[b, h] = decay_grad
         d_all[0, h, pl.ds(pl.multiple_of(b * length, length), length), :] = dv_.astype(BF16)
 
     def weight_term(h):
@@ -239,22 +249,24 @@
         for r in range(1, sp):
             g_copy(r, h).start()
 
-    reach = (outer - 1) * LAG
-    delay = reach + 1
+    delay = (outer - 1) * LAG + 1 + EXTRA
 
     def phase_two(s, _):
+        for side in range(2):
+            at = s - 1 - (z if side == 0 else outer - 1 - z) * LAG
+
+            @pl.when((at >= 0) & (at < units))
+            def _():
+                combine(side, at)
+
         @pl.when(s < units)
         def _():
             h, step = s // own, lax.rem(s, own)
+            low, up = parts(y * own + step, h)
+            a_in[0, 0, s] = low
+            a_in[1, 0, s] = up
             for r in range(inner):
-                intra(r * own + step, h)
-
-        for side in range(2):
-            at = s - (z if side == 0 else outer - 1 - z) * LAG
-
-            @pl.when((at >= 0) & (at < units))
-            def _():
-                combine(side, at)
+                intra(member(r) * own + step, h)
 
         last = s - delay
 
@@ -372,22 +384,22 @@
     outs = pl.pallas_call(
         functools.partial(kernel, dims),
         out_shape=(
-            jax.ShapeDtypeStruct(queries.shape, BF16),
-            jax.ShapeDtypeStruct(queries.shape, BF16),
-            jax.ShapeDtypeStruct(queries.shape, F32),
-            jax.ShapeDtypeStruct(queries.shape, F32),
+            jax.ShapeDtypeStruct((batch, heads, length, pack), BF16),
+            jax.ShapeDtypeStruct((batch, heads, length, pack), F32),
             jax.ShapeDtypeStruct((rows, feat), BF16),
             jax.ShapeDtypeStruct((rows_sp, cols), F32),
         ),
         in_specs=[whole] * 7,
-        out_specs=(whole,) * 6,
+        out_specs=(whole,) * 4,
         scratch_shapes=scratch,
         compiler_params=pltpu.CompilerParams(
             collective_id=0, has_side_effects=True, vmem_limit_bytes=60 * 1024 * 1024
         ),
     )(hidden.reshape(rows, width), value_weight, queries, key_vectors, forward_decay, backward_decay,
       cotangent.reshape(rows, cols))
-    return (outs[0], outs[1], outs[2], outs[3], outs[4].reshape(batch, length, feat), outs[5])
+    near, decays = outs[0], outs[1]
+    return (near[..., :dk], near[..., dk:], decays[..., :dk], decays[..., dk:],
+            outs[2].reshape(batch, length, feat), outs[3])
 
 
 def solution(mesh):

time: 108 us -> 84.9 us (0.79)
  Pallas kernels: 100 us -> 78.2 us
  local copies, waits for them, and re-layouts: 7.31 us -> 5.9 us
    pallas_call x1, Pallas kernels: 100 us -> 78.2 us  [shards(): pl.pallas_call(functools.partial(kernel, dims), out_shape=(jax.ShapeDtype...]
    unnamed x14 -> x8, local copies, waits for them, and re-layouts: 7.31 us -> 1.46 us
    slice x0 -> x2, local copies, waits for them, and re-layouts: none -> 4.44 us  [the longest x1 3.27 us: shards(): decays[..., dk:]]
where the time goes in v2:
time: 84.9 us; the launch traced here: 84.8 us
  Pallas kernels  78.2 us (92%)
  local copies, waits for them, and re-layouts  5.9 us (7%)
    pallas_call x1, Pallas kernels, shards(): pl.pallas_call(functools.partial(kernel, dims), out_shape=(jax.ShapeDtype...  78.2 us
    slice x1, local copies, waits for them, and re-layouts, shards(): decays[..., dk:]  3.27 us

profile of v2, /device:TPU:0, one launch (start us, length us, event | category | flops | bytes accessed | tf_op | source)
XLA Modules:
  0.0 84.8 jit_solution(6639150923735647456)
XLA Ops:
  0.6 78.2 %shard_map.118 = (bf16[16,2,64,128]{3,2,1,0:T(8,128)(2,1)}, f32[16,2,64,128]{3,2,1,0:T(8,128)}, bf16[1024,256]{1,0:T(8,128)(2,1)}, f32[128,256]{1,0:T(8,128)}) custom-call(bf16[1024,1024]{1,0:T(8,128)(2,1)} %bitcast.3, bf16[1024,256]{1,0:T(8,128)(2,1)} %wgt.1, bf16[16,2,64,64]{3,2,1,0:T(8,128)(2,1)} %qry.1, bf16[16,2,64,64]{3,2,1,0:T(8,128)(2,1)} %key.1, ...), custom_call_target="tpu_custom_call" | custom-call | tf_op jit(solution)/shard_map/pallas_call | solution.py:384
  78.8 0.0 copy-start
  78.8 3.3 %fusion = (f32[16,2,64,64]{3,2,1,0:T(8,128)}, f32[16,2,64,64]{3,2,1,0:T(8,128)}) fusion(f32[16,2,64,128]{3,2,1,0:T(8,128)} %get-tuple-element.11), kind=kLoop, calls=%fused_computation | loop fusion | bytes 2097152 | tf_op jit(solution)/shard_map/slice | solution.py:401
  82.1 0.0 copy-start.1
  82.1 0.0 copy-start.2
  82.1 0.0 copy-done
  82.1 1.2 %fusion.1 = (bf16[16,2,64,64]{3,2,1,0:T(8,128)(2,1)}, bf16[16,2,64,64]{3,2,1,0:T(8,128)(2,1)}) fusion(bf16[16,2,64,128]{3,2,1,0:T(8,128)(2,1)S(1)} %copy-done), kind=kLoop, calls=%fused_computation.1 | loop fusion | bytes 1048576 | tf_op jit(solution)/shard_map/slice | solution.py:401
  83.3 0.0 copy-done.1
  83.3 0.8 copy.15
  84.1 0.0 copy-done.2
  84.1 0.7 copy.16
Async XLA Ops:
  78.8 3.3 %copy-start = (bf16[16,2,64,128]{3,2,1,0:T(8,128)(2,1)S(1)}, bf16[16,2,64,128]{3,2,1,0:T(8,128)(2,1)}, u32[]{:S(2)}) copy-start(bf16[16,2,64,128]{3,2,1,0:T(8,128)(2,1)} %get-tuple-element.10) | copy-start | bytes 1572868
  82.1 1.2 %copy-start.1 = (bf16[1024,256]{1,0:T(8,128)(2,1)S(1)}, bf16[1024,256]{1,0:T(8,128)(2,1)}, u32[]{:S(2)}) copy-start(bf16[1024,256]{1,0:T(8,128)(2,1)} %get-tuple-element.12) | copy-start | bytes 1572868
  82.1 2.0 %copy-start.2 = (f32[128,256]{1,0:T(8,128)S(1)}, f32[128,256]{1,0:T(8,128)}, u32[]{:S(2)}) copy-start(f32[128,256]{1,0:T(8,128)} %get-tuple-element.29) | copy-start | bytes 393220
